TPU v7x, 32 devices: a whole 2x2x4 slice. The times are simulated.
32 devices in a mesh: sp: 4 (over x, core), dp: 8 (over z, y).
Axes of the slice: x: 2, y: 2, z: 4, core: 2. Of those that a mesh axis runs over, the one named last changes fastest.
Arguments:
- query: bfloat16 [8, 512, 1024], P('dp', None, 'sp'), may hold values from -120 to 120
- keys: bfloat16 [8, 512, 1024], P('dp', None, 'sp'), may hold values from -6 to 6
- values: bfloat16 [8, 512, 1024], P('dp', None, 'sp'), may hold values from -6 to 6
- output: bfloat16 [8, 512, 1024], P('dp'), may hold values from -1 to 1
- cum: float32 [8, 16, 512], P('dp', 'sp'), as said below
- d_out: bfloat16 [8, 512, 2048], P('dp', 'sp'), may hold values from -6 to 6
- w_out: bfloat16 [1024, 2048], P('dp'), may hold values from -0.125 to 0.125
Outputs:
- d_query: bfloat16 [8, 512, 1024], P('dp', 'sp')
- d_key: bfloat16 [8, 512, 1024], P('dp', 'sp')
- d_value: bfloat16 [8, 512, 1024], P('dp', 'sp')
- d_cum: float32 [8, 16, 512], P('dp', 'sp')
- d_w_out: float32 [1024, 2048], P('dp', 'sp')
Inputs may be any that keep to these rules, and one draw needn't show every extreme that they name: cum never rises along positions.
All inputs are finite; a program needn't handle non-finite values.
Results may differ from a plain program's by a relative error of at most 0.008.
Values may be sent and summed in bfloat16 or wider, within the bound.
No kernel may reach another device: no remote copies, remote signals or barrier semaphores. Data moves between devices by JAX's collectives and lax.ppermute only.
A program may use at most 64 MiB of HBM per device.

v0:
```python
import jax
import jax.numpy as jnp
from jax import lax
from jax.sharding import PartitionSpec as P


def head_grads(query, keys, values, output, cotangent, cum):
    head_count, length, head_width = query.shape
    span_rows = min(512, length)
    score_scale = head_width ** (-0.5)
    row_dots = jnp.sum(cotangent.astype(jnp.float32) * output.astype(jnp.float32), axis=2)
    positions = jnp.arange(length)

    def product(left, right, form):
        return jnp.einsum(form, left, right, preferred_element_type=jnp.float32)

    def advance(totals, block_index):
        key_grad, value_grad, cum_grad = totals
        offset = block_index * span_rows
        query_blk = lax.dynamic_slice_in_dim(query, offset, span_rows, 1)
        cot_blk = lax.dynamic_slice_in_dim(cotangent, offset, span_rows, 1)
        cum_blk = lax.dynamic_slice_in_dim(cum, offset, span_rows, 1)
        dots_blk = lax.dynamic_slice_in_dim(row_dots, offset, span_rows, 1)
        scores = product(query_blk, keys, "hqe,hke->hqk") * score_scale
        scores = scores + cum_blk[:, :, None] - cum[:, None, :]
        query_pos = offset + jnp.arange(span_rows)
        causal = positions[None, :] <= query_pos[:, None]
        scores = jnp.where(causal[None], scores, -1e30)
        row_max = jnp.max(scores, axis=2, keepdims=True)
        weights = jnp.exp(scores - row_max)
        weights = weights / jnp.sum(weights, axis=2, keepdims=True)
        weights_b = weights.astype(jnp.bfloat16)
        d_prob = product(cot_blk, values, "hqe,hke->hqk")
        d_score = weights * (d_prob - dots_blk[:, :, None])
        score_b = d_score.astype(jnp.bfloat16)
        query_grad = (product(score_b, keys, "hqk,hke->hqe") * score_scale).astype(jnp.bfloat16)
        key_grad = key_grad + product(score_b, query_blk, "hqk,hqe->hke") * score_scale
        value_grad = value_grad + product(weights_b, cot_blk, "hqk,hqe->hke")
        cum_grad = cum_grad - jnp.sum(d_score, axis=1)
        own_part = lax.dynamic_slice_in_dim(cum_grad, offset, span_rows, 1) + jnp.sum(
            d_score, axis=2
        )
        cum_grad = lax.dynamic_update_slice_in_dim(cum_grad, own_part, offset, 1)
        return ((key_grad, value_grad, cum_grad), query_grad)

    start_state = (
        jnp.zeros(query.shape, jnp.float32),
        jnp.zeros(query.shape, jnp.float32),
        jnp.zeros(cum.shape, jnp.float32),
    )
    totals, query_blocks = lax.scan(advance, start_state, jnp.arange(length // span_rows))
    query_grad = jnp.transpose(query_blocks, (1, 0, 2, 3)).reshape(query.shape)
    return (query_grad, totals[0].astype(jnp.bfloat16), totals[1].astype(jnp.bfloat16), totals[2])


def shards(query, keys, values, output, cum, d_out, w_out):
    local_rows = d_out[0]
    whole_output = output[0]
    d_attn = lax.dot_general(
        local_rows,
        lax.all_gather(w_out, "dp", axis=0, tiled=True),
        (((1,), (1,)), ((), ())),
        preferred_element_type=jnp.float32,
    ).astype(jnp.bfloat16)
    head_cot, column_part = (
        lax.all_to_all(d_attn[None], "sp", split_axis=2, concat_axis=1, tiled=True),
        lax.all_to_all(d_out, "sp", split_axis=2, concat_axis=1, tiled=True),
    )
    grad_weight = lax.psum_scatter(
        lax.dot_general(
            whole_output,
            column_part[0],
            (((0,), (0,)), ((), ())),
            preferred_element_type=jnp.float32,
        ),
        "dp",
        scatter_dimension=0,
        tiled=True,
    )
    head_cols = query.shape[2]
    head_count = cum.shape[1]
    head_width = head_cols // head_count
    seq_length = query.shape[1]
    own_output = lax.dynamic_slice_in_dim(
        whole_output, lax.axis_index("sp") * head_cols, head_cols, 1
    )

    def heads_first(matrix):
        return jnp.transpose(matrix.reshape(seq_length, head_count, head_width), (1, 0, 2))

    def tokens_first(matrix):
        return jnp.transpose(matrix, (1, 0, 2)).reshape(1, seq_length, head_cols)

    grads = head_grads(
        heads_first(query[0]),
        heads_first(keys[0]),
        heads_first(values[0]),
        heads_first(own_output),
        heads_first(head_cot[0]),
        cum[0],
    )
    query_grad, key_grad, value_grad = (
        lax.all_to_all(tokens_first(grads[0]), "sp", split_axis=1, concat_axis=2, tiled=True),
        lax.all_to_all(tokens_first(grads[1]), "sp", split_axis=1, concat_axis=2, tiled=True),
        lax.all_to_all(tokens_first(grads[2]), "sp", split_axis=1, concat_axis=2, tiled=True),
    )
    return (query_grad, key_grad, value_grad, grads[3][None], grad_weight)


def solution(mesh):
    placed = (
        P("dp", None, "sp"),
        P("dp", None, "sp"),
        P("dp", None, "sp"),
        P("dp", None, None),
        P("dp", "sp", None),
        P("dp", "sp", None),
        P("dp", None),
    )
    return jax.shard_map(
        shards,
        mesh=mesh,
        in_specs=placed,
        out_specs=(
            P("dp", "sp", None),
            P("dp", "sp", None),
            P("dp", "sp", None),
            P("dp", "sp", None),
            P("dp", "sp"),
        ),
        check_vma=False,
    )
```

profile of v0, /device:TPU:0, one launch (start us, length us, event | category | flops | bytes accessed | tf_op | source)
XLA Modules:
  0.0 163.5 jit_solution(12182984740562545491)
XLA Ops:
  7.2 0.7 all-gather.2.cloned.1.call-update
  7.9 2.4 %copy.99 = bf16[1,128,2048]{1,0,2:T(2,128)(2,1)S(1)} copy(bf16[1,128,2048]{2,1,0:T(8,128)(2,1)} %param.12) | data formatting | bytes 1048576 | tf_op args[5]
  10.8 11.5 %reduce.4 = bf16[2048,128]{1,0:T(8,128)(2,1)S(1)} reduce(bf16[2048,1,128]{2,1,0:T(2,128)(2,1)S(1)} %bitcast.83, bf16[]{:T(256)} %broadcast.48), dimensions={1}, to_apply=%bitcast.67.reduce_sub_computation | reduce | bytes 1048578
  22.5 12.9 %all_to_all.84 = bf16[4,2,32768]{2,1,0:T(2,128)(2,1)S(1)} all-to-all(bf16[4,2,32768]{2,1,0:T(2,128)(2,1)S(1)} %reshape.79), channel_id=1, replica_groups=mesh['sp'=4,'dp'=8] {'sp'}, dimensions={0} | all-to-all | bytes 1048576 | tf_op jit(solution)/shard_map/all_to_all | solution.py:67
  36.2 2.1 %fusion.15 = f32[1024,512]{1,0:T(8,128)} fusion(bf16[512,512]{1,0:T(8,128)(2,1)S(1)} %bitcast.85, bf16[1,512,1024]{2,1,0:T(8,128)(2,1)S(1)} %copy-done.1), kind=kOutput, calls=%fused_computation.20 | convolution fusion | flops 536870912 | bytes 3670016 | tf_op jit(solution)/shard_map/dot_general | solution.py:70
  38.9 0.8 copy.87
  39.9 45.8 %all-gather.2.cloned.1.call-done = bf16[1024,2048]{1,0:T(8,128)(2,1)} async-done(((bf16[128,2048]{1,0:T(8,128)(2,1)}), bf16[1024,2048]{1,0:T(8,128)(2,1)}) %all-gather.2.cloned.1.call-update) | async-done | bytes 4194320 | tf_op jit(solution)/shard_map/all_gather | solution.py:61
  85.7 3.7 %fusion.14 = bf16[1,128,1024]{2,1,0:T(8,128)(2,1)S(1)} fusion(bf16[1024,2048]{1,0:T(8,128)(2,1)} %all-gather.2.cloned.1.call-done, bf16[1,128,2048]{2,1,0:T(8,128)(2,1)S(1)} %copy-done), kind=kOutput, calls=%fused_computation.19 | convolution fusion | flops 537001984 | bytes 4980736 | tf_op jit(solution)/shard_map/dot_general | solution.py:59
  89.8 2.2 %reduce = bf16[1024,128]{1,0:T(8,128)(2,1)S(1)} reduce(bf16[1024,1,128]{2,1,0:T(2,128)(2,1)S(1)} %bitcast.92, bf16[]{:T(256)} %broadcast.48), dimensions={1}, to_apply=%bitcast.59.reduce_sub_computation | reduce | bytes 524290
  92.0 0.8 reshape.71
  92.8 3.6 %all-to-all-start = ((bf16[4,2,16384]{2,1,0:T(2,128)(2,1)}), bf16[4,2,16384]{2,1,0:T(2,128)(2,1)S(1)}, u32[]{:S(2)}, u32[]{:S(2)}) async-start(bf16[4,2,16384]{2,1,0:T(2,128)(2,1)} %reshape.71), calls=%async_computation | async-start | bytes 524288 | tf_op jit(solution)/shard_map/all_to_all | solution.py:66
  96.4 3.4 %fusion.32 = (f32[4,512]{1,0:T(4,128)S(1)}, f32[4,512,512]{1,2,0:T(8,128)}) fusion(f32[4,512]{1,0:T(4,128)S(1)} %bitcast.112, pred[512,512]{0,1:T(8,128)(4,1)S(1)} %iota_compare_fusion, bf16[4,512,64]{1,2,0:T(8,128)(2,1)S(1)} %bitcast.97, bf16[4,512,64]{1,2,0:T(8,128)(2,1)S(1)} %bitcast.100), kind=kOutput, calls=%fused_computation.38 | convolution fusion | flops 140509696 | bytes 4997120 | tf_op jit(solution)/shard_map/while/body/eval_jaxpr/sub | solution.py:30
  99.8 2.3 %all-to-all-done = bf16[4,2,16384]{2,1,0:T(2,128)(2,1)S(1)} async-done(((bf16[4,2,16384]{2,1,0:T(2,128)(2,1)}), bf16[4,2,16384]{2,1,0:T(2,128)(2,1)S(1)}, u32[]{:S(2)}, u32[]{:S(2)}) %all-to-all-start) | async-done | bytes 262176 | tf_op jit(solution)/shard_map/all_to_all | solution.py:66
  102.9 3.5 %fusion.31 = (f32[4,512]{1,0:T(4,128)S(1)}, f32[4,512]{1,0:T(4,128)S(1)}, bf16[4,512,512]{1,2,0:T(8,128)(2,1)S(1)}) fusion(f32[4,512]{1,0:T(4,128)S(1)} %multiply_reduce_fusion, bf16[4,512,64]{1,2,0:T(8,128)(2,1)} %bitcast.111, bf16[512,4,64]{0,2,1:T(8,128)(2,1)S(1)} %reshape_squeeze.14, f32[4,512,512]{1,2,0:T(8,128)} %get-tuple-element.52, ...), kind=kOutput, calls=%fused_computation.37 | convolution fusion | flops 140505088 | bytes 6848512 | tf_op jit(solution)/shard_map/while/body/eval_jaxpr/hqe,hke->hqk/dot_general | solution.py:15
  106.4 0.8 fusion.9
  107.6 3.0 %reduce.2 = bf16[512,256]{1,0:T(8,128)(2,1)} reduce(bf16[512,1,256]{2,1,0:T(2,128)(2,1)S(1)} %bitcast.93, bf16[]{:T(256)} %broadcast.48), dimensions={1}, to_apply=%bitcast.63.reduce_sub_computation | reduce | bytes 524290
  110.6 1.7 %reshape.75 = bf16[4,2,16384]{2,1,0:T(2,128)(2,1)} reshape(bf16[512,256]{1,0:T(8,128)(2,1)} %reduce.2) | data formatting | bytes 524288
  112.3 3.4 %all-to-all-start.2 = ((bf16[4,2,16384]{2,1,0:T(2,128)(2,1)}), bf16[4,2,16384]{2,1,0:T(2,128)(2,1)S(1)}, u32[]{:S(2)}, u32[]{:S(2)}) async-start(bf16[4,2,16384]{2,1,0:T(2,128)(2,1)} %reshape.75), calls=%async_computation.2 | async-start | bytes 524288 | tf_op jit(solution)/shard_map/all_to_all | solution.py:104
  116.6 2.2 %reduce.1 = bf16[512,256]{1,0:T(8,128)(2,1)S(1)} reduce(bf16[512,1,256]{2,1,0:T(2,128)(2,1)S(1)} %bitcast.94, bf16[]{:T(256)} %broadcast.48), dimensions={1}, to_apply=%bitcast.61.reduce_sub_computation | reduce | bytes 524290
  118.8 0.8 reshape.73
  119.6 2.1 %all-to-all-done.2 = bf16[4,2,16384]{2,1,0:T(2,128)(2,1)S(1)} async-done(((bf16[4,2,16384]{2,1,0:T(2,128)(2,1)}), bf16[4,2,16384]{2,1,0:T(2,128)(2,1)S(1)}, u32[]{:S(2)}, u32[]{:S(2)}) %all-to-all-start.2) | async-done | bytes 262176 | tf_op jit(solution)/shard_map/all_to_all | solution.py:104
  121.7 3.4 %all-to-all-start.1 = ((bf16[4,2,16384]{2,1,0:T(2,128)(2,1)}), bf16[4,2,16384]{2,1,0:T(2,128)(2,1)S(1)}, u32[]{:S(2)}, u32[]{:S(2)}) async-start(bf16[4,2,16384]{2,1,0:T(2,128)(2,1)} %reshape.73), calls=%async_computation.1 | async-start | bytes 524288 | tf_op jit(solution)/shard_map/all_to_all | solution.py:103
  125.1 3.2 %fusion.11 = bf16[4,512,64]{1,2,0:T(8,128)(2,1)S(1)} fusion(f32[4,512]{1,0:T(4,128)S(1)} %get-tuple-element.38, bf16[512,4,64]{0,2,1:T(8,128)(2,1)S(1)} %copy-done.3, f32[4,512]{1,0:T(4,128)S(1)} %bitcast.113, pred[512,512]{0,1:T(8,128)(4,1)} %copy-done.7, bf16[4,512,64]{1,2,0:T(8,128)(2,1)S(1)} %bitcast.99, bf16[4,512,64]{1,2,0:T(8,128)(2,1)S(1)} %bitcast.102), kind=kOutput, calls=%fused_computation.18 | convolution fusion | flops 275909120 | bytes 1327104 | tf_op jit(solution)/shard_map/while/body/eval_jaxpr/hqk,hqe->hke/dot_general | solution.py:15
  128.8 2.2 %reduce.3 = bf16[512,256]{1,0:T(8,128)(2,1)S(1)} reduce(bf16[512,1,256]{2,1,0:T(2,128)(2,1)S(1)} %bitcast.91, bf16[]{:T(256)} %broadcast.48), dimensions={1}, to_apply=%bitcast.65.reduce_sub_computation | reduce | bytes 524290
  131.0 0.8 reshape.77
  131.7 3.4 %all-to-all-start.3 = ((bf16[4,2,16384]{2,1,0:T(2,128)(2,1)}), bf16[4,2,16384]{2,1,0:T(2,128)(2,1)S(1)}, u32[]{:S(2)}, u32[]{:S(2)}) async-start(bf16[4,2,16384]{2,1,0:T(2,128)(2,1)} %reshape.77), calls=%async_computation.3 | async-start | bytes 524288 | tf_op jit(solution)/shard_map/all_to_all | solution.py:105
  135.2 0.6 add_bitcast_fusion
  136.3 0.9 copy.102
  137.6 0.9 copy.101
  138.5 2.7 %all-to-all-done.3 = bf16[4,2,16384]{2,1,0:T(2,128)(2,1)S(1)} async-done(((bf16[4,2,16384]{2,1,0:T(2,128)(2,1)}), bf16[4,2,16384]{2,1,0:T(2,128)(2,1)S(1)}, u32[]{:S(2)}, u32[]{:S(2)}) %all-to-all-start.3) | async-done | bytes 262176 | tf_op jit(solution)/shard_map/all_to_all | solution.py:105
  141.6 0.9 copy.103
  142.5 14.2 %reduce-scatter.2.cloned.1.call-done = f32[128,512]{1,0:T(8,128)} async-done(((f32[1024,512]{1,0:T(8,128)}), f32[128,512]{1,0:T(8,128)}) %reduce-scatter.2.cloned.1.call-update) | async-done | bytes 262160 | tf_op jit(solution)/shard_map/reduce_scatter | solution.py:69
  (51 shorter events, 6.5 us)
Async XLA Ops:
  7.2 78.5 %all-gather.2.cloned.1.call-start = ((), (), s32[]{:S(2)}) async-start(), calls=%async_computation.6 | async-start | bytes 4718592 | tf_op jit(solution)/shard_map/all_gather | solution.py:61
  7.9 148.7 %reduce-scatter.2.cloned.1.call-start = ((), (), s32[]{:S(2)}) async-start(), calls=%async_computation.7 | async-start | bytes 2359296 | tf_op jit(solution)/shard_map/reduce_scatter | solution.py:69
  10.3 25.9 %copy-start.1 = (bf16[1,512,1024]{2,1,0:T(8,128)(2,1)S(1)}, bf16[1,512,1024]{2,1,0:T(8,128)(2,1)}, u32[]{:S(2)}) copy-start(bf16[1,512,1024]{2,1,0:T(8,128)(2,1)} %param.10) | copy-start | bytes 3145732
  35.9 2.6 %copy-start.4 = (bf16[1,512,256]{2,1,0:T(8,128)(2,1)S(1)}, bf16[1,512,256]{2,1,0:T(8,128)(2,1)}, u32[]{:S(2)}) copy-start(bf16[1,512,256]{2,1,0:T(8,128)(2,1)} %param.7) | copy-start | bytes 786436
  36.2 2.6 %copy-start.5 = (bf16[1,512,256]{2,1,0:T(8,128)(2,1)S(1)}, bf16[1,512,256]{2,1,0:T(8,128)(2,1)}, u32[]{:S(2)}) copy-start(bf16[1,512,256]{2,1,0:T(8,128)(2,1)} %param.8) | copy-start | bytes 786436
  36.2 2.7 %copy-start.6 = (bf16[1,512,256]{2,1,0:T(8,128)(2,1)S(1)}, bf16[1,512,256]{2,1,0:T(8,128)(2,1)}, u32[]{:S(2)}) copy-start(bf16[1,512,256]{2,1,0:T(8,128)(2,1)} %param.9) | copy-start | bytes 786436
  36.2 49.5 %copy-start = (bf16[1,128,2048]{2,1,0:T(8,128)(2,1)S(1)}, bf16[1,128,2048]{2,1,0:T(8,128)(2,1)}, u32[]{:S(2)}) copy-start(bf16[1,128,2048]{2,1,0:T(8,128)(2,1)} %param.12) | copy-start | bytes 1572868
  38.9 57.5 %copy-start.8 = (f32[1,4,512]{2,1,0:T(4,128)S(1)}, f32[1,4,512]{2,1,0:T(4,128)}, u32[]{:S(2)}) copy-start(f32[1,4,512]{2,1,0:T(4,128)} %param.11) | copy-start | bytes 24580
  39.9 60.0 %copy-start.7 = (pred[512,512]{0,1:T(8,128)(4,1)}, pred[512,512]{0,1:T(8,128)(4,1)S(1)}, u32[]{:S(2)}) copy-start(pred[512,512]{0,1:T(8,128)(4,1)S(1)} %iota_compare_fusion) | copy-start | bytes 786436
  92.8 9.4 %all-to-all-start = ((bf16[4,2,16384]{2,1,0:T(2,128)(2,1)}), bf16[4,2,16384]{2,1,0:T(2,128)(2,1)S(1)}, u32[]{:S(2)}, u32[]{:S(2)}) async-start(bf16[4,2,16384]{2,1,0:T(2,128)(2,1)} %reshape.71), calls=%async_computation | async-start | bytes 524288 | tf_op jit(solution)/shard_map/all_to_all | solution.py:66
  102.8 3.6 %copy-start.2 = (bf16[512,4,64]{0,2,1:T(8,128)(2,1)}, bf16[512,4,64]{0,2,1:T(8,128)(2,1)S(1)}, u32[]{:S(2)}) copy-start(bf16[512,4,64]{0,2,1:T(8,128)(2,1)S(1)} %reshape_squeeze.14) | copy-start | bytes 786436
  107.6 17.5 %copy-start.3 = (bf16[512,4,64]{0,2,1:T(8,128)(2,1)S(1)}, bf16[512,4,64]{0,2,1:T(8,128)(2,1)}, u32[]{:S(2)}) copy-start(bf16[512,4,64]{0,2,1:T(8,128)(2,1)} %copy-done.2) | copy-start | bytes 786436
  112.3 9.4 %all-to-all-start.2 = ((bf16[4,2,16384]{2,1,0:T(2,128)(2,1)}), bf16[4,2,16384]{2,1,0:T(2,128)(2,1)S(1)}, u32[]{:S(2)}, u32[]{:S(2)}) async-start(bf16[4,2,16384]{2,1,0:T(2,128)(2,1)} %reshape.75), calls=%async_computation.2 | async-start | bytes 524288 | tf_op jit(solution)/shard_map/all_to_all | solution.py:104
  121.7 10.1 %all-to-all-start.1 = ((bf16[4,2,16384]{2,1,0:T(2,128)(2,1)}), bf16[4,2,16384]{2,1,0:T(2,128)(2,1)S(1)}, u32[]{:S(2)}, u32[]{:S(2)}) async-start(bf16[4,2,16384]{2,1,0:T(2,128)(2,1)} %reshape.73), calls=%async_computation.1 | async-start | bytes 524288 | tf_op jit(solution)/shard_map/all_to_all | solution.py:103
  131.7 9.4 %all-to-all-start.3 = ((bf16[4,2,16384]{2,1,0:T(2,128)(2,1)}), bf16[4,2,16384]{2,1,0:T(2,128)(2,1)S(1)}, u32[]{:S(2)}, u32[]{:S(2)}) async-start(bf16[4,2,16384]{2,1,0:T(2,128)(2,1)} %reshape.77), calls=%async_computation.3 | async-start | bytes 524288 | tf_op jit(solution)/shard_map/all_to_all | solution.py:105
Sparse Core Ops, SparseCore 0:
  10.1 75.5 all-gather.1
  89.8 66.8 reduce-scatter.1
where the time goes:
time: 164 us; the launch traced here: 163 us
  waiting for transfers between devices  67.7 us (41%)
  other arithmetic  21.9 us (13%)
  matrix products  17.1 us (10%)
  local copies, waits for them, and re-layouts  15.5 us (9%)
  between operations  14.5 us (9%)
  starting transfers between devices  13.9 us (8%)
  blocking collectives  12.9 us (8%)
    all_gather x1, waiting for transfers between devices, shards(): lax.all_gather(w_out, 'dp', axis=0, tiled=True)  45.8 us
    unnamed x5, other arithmetic  21.1 us
    reduce_scatter x1, waiting for transfers between devices, shards(): lax.psum_scatter(lax.dot_general(whole_output, column_part[0], (((0,), (0...  14.2 us
    all_to_all x1, blocking collectives, shards(): lax.all_to_all(d_out, 'sp', split_axis=2, concat_axis=1, tiled=True)  12.9 us
    unnamed x41, local copies, waits for them, and re-layouts  12.5 us
    dot_general x4, matrix products, product(): return jnp.einsum(form, left, right, preferred_element_type=jnp.float32)  7.92 us
    dot_general x1, matrix products, shards(): lax.dot_general(local_rows, lax.all_gather(w_out, 'dp', axis=0, tiled=Tru...  3.7 us
    all_to_all x1, starting transfers between devices, shards(): lax.all_to_all(d_attn[None], 'sp', split_axis=2, concat_axis=1, tiled=True)  3.6 us
  transfers between devices with their start and end apart: 6, of which 5 were waited for; matrix products, arithmetic and copies ran while one was open for 33% of the time, Pallas kernels for 0%

commit v1 on v0

--- a/solution.py
+++ b/solution.py
@@ -1,7 +1,288 @@
+import functools
+
 import jax
 import jax.numpy as jnp
 from jax import lax
+from jax.experimental import pallas as pl
+from jax.experimental.pallas import tpu as pltpu
 from jax.sharding import PartitionSpec as P
+
+LANES = 128
+F32 = jnp.float32
+BF16 = jnp.bfloat16
+
+
+def dot_nn(left, right):
+    return lax.dot_general(left, right, (((1,), (0,)), ((), ())), preferred_element_type=F32)
+
+
+def dot_nt(left, right):
+    return lax.dot_general(left, right, (((1,), (1,)), ((), ())), preferred_element_type=F32)
+
+
+def window(index, size):
+    return pl.ds(pl.multiple_of(index * size, size), size)
+
+
+def lane_head(value, head, width):
+    lane = lax.broadcasted_iota(jnp.int32, value.shape, 1)
+    inside = (lane >= head * width) & (lane < (head + 1) * width)
+    return jnp.where(inside, value, jnp.zeros_like(value))
+
+
+def row_head(value, head, width):
+    row = lax.broadcasted_iota(jnp.int32, value.shape, 0)
+    inside = (row >= head * width) & (row < (head + 1) * width)
+    return jnp.where(inside, value, jnp.zeros_like(value))
+
+
+def prob_kernel(heads, query_ref, keys_ref, output_ref, cum_ref, prob_ref, out_t_ref, keys_t_ref):
+    length, width = query_ref.shape
+    head_width = width // heads
+    per_group = LANES // head_width
+    scale = jnp.asarray(head_width**-0.5, BF16)
+    cum = cum_ref[...]
+    cum_cols = jnp.transpose(jnp.concatenate([cum] + [jnp.zeros_like(cum)] * (8 // heads - 1), 0))
+    key_at = lax.broadcasted_iota(jnp.int32, (LANES, LANES), 0)
+    query_at = lax.broadcasted_iota(jnp.int32, (LANES, LANES), 1)
+    causal = key_at <= query_at
+    for head in range(heads):
+        lanes = pl.ds(head // per_group * LANES, LANES)
+        keys_head = lane_head(keys_ref[:, lanes], head % per_group, head_width)
+        cum_key = cum_cols[:, head : head + 1]
+        for block in range(length // LANES):
+            rows = (block + 1) * LANES
+            own = pl.ds(block * LANES, LANES)
+            scores = dot_nt(keys_head[:rows], query_ref[own, lanes] * scale)
+            scores = scores + cum[head : head + 1, block * LANES : rows] - cum_key[:rows]
+            last = jnp.where(causal, scores[block * LANES :], -1e30)
+            scores = jnp.concatenate([scores[: block * LANES], last], 0) if block else last
+            weights = jnp.exp(scores - jnp.max(scores, axis=0, keepdims=True))
+            weights = weights * (1.0 / jnp.sum(weights, axis=0, keepdims=True))
+            prob_ref[head, :rows, own] = weights.astype(BF16)
+    out_t_ref[...] = jnp.transpose(output_ref[...])
+    keys_t_ref[...] = jnp.transpose(keys_ref[...] * scale)
+
+
+def weight_kernel(inner, *refs):
+    out_t_ref, shards, (keep_ref, send_ref, columns_ref) = refs[0], refs[1:-3], refs[-3:]
+    me, place = lax.axis_index("sp"), lax.axis_index("dp")
+    outer, mine = place // inner, place % inner
+    tokens = shards[0].shape[0]
+    slots, block_rows, width = keep_ref.shape
+    for step, shard in enumerate(shards):
+        columns_ref[window(me ^ step, tokens), :] = shard[:, window(me, width)]
+    columns = columns_ref[...]
+    for slot in range(slots):
+        target = (outer + slot) % slots
+        keep = out_t_ref[window(target * inner + mine, block_rows), :]
+        send = out_t_ref[window(target * inner + (mine ^ 1), block_rows), :]
+        keep_ref[slot] = dot_nn(keep, columns)
+        send_ref[slot] = dot_nn(send, columns).astype(BF16)
+
+
+def merge_kernel(keep_ref, got_ref, own_ref, *send_refs):
+    own_ref[...] = keep_ref[0] + got_ref[0].astype(F32)
+    for slot, send_ref in enumerate(send_refs, 1):
+        send_ref[...] = (keep_ref[slot] + got_ref[slot].astype(F32)).astype(BF16)
+
+
+def finish_kernel(own_ref, *refs):
+    total = own_ref[...]
+    for got_ref in refs[:-1]:
+        total = total + got_ref[...].astype(F32)
+    refs[-1][...] = total
+
+
+def grads_kernel(other, heads, steps, pieces, *refs):
+    (prob_ref, query_ref, keys_t_ref, values_ref, out_t_ref), refs = refs[:5], refs[5:]
+    shards, refs = refs[:steps], refs[steps:]
+    weights, refs = refs[:pieces], refs[pieces:]
+    slot_refs, refs = refs[:steps], refs[steps:]
+    cum_ref, cot_ref, score_ref, query_grad_ref, key_grad_ref, value_grad_ref, sums_ref = refs
+    me = lax.axis_index("sp")
+    group = lax.axis_index("dp") % 2
+    if other:
+        group = 1 - group
+    length, width = query_ref.shape
+    head_width = width // heads
+    per_group = LANES // head_width
+    tokens = shards[0].shape[0]
+    scale = jnp.asarray(head_width**-0.5, BF16)
+    weight = jnp.concatenate([piece[...] for piece in weights], 0)
+    for step, shard in enumerate(shards):
+        cot_ref[:, window(me ^ step, tokens)] = dot_nt(weight, shard[...]).astype(BF16)
+    lanes = window(group, LANES)
+    cot = cot_ref[...]
+    query = query_ref[:, lanes] * scale
+    keys_t = keys_t_ref[lanes, :]
+    out_t = out_t_ref[window(me * (width // LANES) + group, LANES), :]
+    product = cot.astype(F32) * out_t.astype(F32)
+    blocks = length // LANES
+    key_grads, value_grads = [0.0] * blocks, [0.0] * blocks
+    query_grads = [0.0] * blocks
+    sum_columns, sum_rows = [], []
+    for head in range(per_group):
+        index = group * per_group + head
+        cot_head = row_head(cot, head, head_width)
+        query_head = lane_head(query, head, head_width)
+        keys_head = row_head(keys_t, head, head_width)
+        dots = jnp.sum(product[head * head_width : (head + 1) * head_width], axis=0, keepdims=True)
+        rows_sum = []
+        for block in range(blocks):
+            rows = (block + 1) * LANES
+            own = pl.ds(block * LANES, LANES)
+            at = slice(block * LANES, rows)
+            d_prob = dot_nn(values_ref[:rows, lanes], cot_head[:, at])
+            d_score = prob_ref[index, :rows, own].astype(F32) * (d_prob - dots[:, at])
+            rows_sum.append(jnp.sum(d_score, axis=0, keepdims=True))
+            if block:
+                sums_ref[: block * LANES, :] += d_score[: block * LANES]
+            sums_ref[own, :] = d_score[block * LANES :]
+            rounded = d_score.astype(BF16)
+            score_ref[:rows, own] = rounded
+            query_grads[block] += dot_nn(keys_head[:, :rows], rounded)
+        for block in range(blocks):
+            own = pl.ds(block * LANES, LANES)
+            start = block * LANES
+            key_grads[block] += dot_nn(score_ref[own, start:], query_head[start:])
+            value_grads[block] += dot_nt(prob_ref[index, own, start:], cot_head[:, start:])
+        sum_columns.append(jnp.sum(sums_ref[...], axis=1, keepdims=True))
+        sum_rows.append(jnp.concatenate(rows_sum, 1))
+    lane = lax.broadcasted_iota(jnp.int32, (length, LANES), 1)
+    spread = jnp.zeros((length, LANES), F32)
+    for head in range(per_group):
+        spread = jnp.where(lane == head, sum_columns[head], spread)
+    cum_ref[...] = jnp.concatenate(sum_rows, 0) - jnp.transpose(spread)[:per_group]
+    for block in range(blocks):
+        own = pl.ds(block * LANES, LANES)
+        query_grad_ref[own, :] = jnp.transpose(query_grads[block]).astype(BF16)
+        key_grad_ref[own, :] = key_grads[block].astype(BF16)
+        value_grad_ref[own, :] = value_grads[block].astype(BF16)
+    for step, slot_ref in enumerate(slot_refs):
+        here = window(me ^ step, tokens)
+        slot_ref[0] = query_grad_ref[here, :]
+        slot_ref[1] = key_grad_ref[here, :]
+        slot_ref[2] = value_grad_ref[here, :]
+
+
+def place_kernel(steps, *refs):
+    first, second = refs[:steps], refs[steps : 2 * steps]
+    first_cum_ref, second_cum_ref = refs[2 * steps : 2 * steps + 2]
+    grad_refs, cum_ref = refs[2 * steps + 2 : -1], refs[-1]
+    me, mine = lax.axis_index("sp"), lax.axis_index("dp") % 2
+    for step in range(steps):
+        for group, parts in ((mine, first), (1 - mine, second)):
+            columns = window((me ^ step) * 2 + group, LANES)
+            for kind, grad_ref in enumerate(grad_refs):
+                grad_ref[:, columns] = parts[step][kind]
+    low, high = first_cum_ref[...], second_cum_ref[...]
+    swap = jnp.full(low.shape, mine, jnp.int32) == 1
+    cum_ref[...] = jnp.concatenate(
+        [jnp.where(swap, high, low), jnp.where(swap, low, high)], 0
+    )
+
+
+def call(kernel, outs, args, scratch=()):
+    return pl.pallas_call(
+        kernel,
+        out_shape=[jax.ShapeDtypeStruct(shape, kind) for shape, kind in outs],
+        in_specs=[pl.BlockSpec(memory_space=pltpu.VMEM)] * len(args),
+        out_specs=[pl.BlockSpec(memory_space=pltpu.VMEM)] * len(outs),
+        scratch_shapes=[pltpu.VMEM(shape, kind) for shape, kind in scratch],
+    )(*args)
+
+
+def fused_shards(sizes, query, keys, values, output, cum, d_out, w_out):
+    split, groups = sizes
+    inner = groups // split
+    query, keys, values, output, cum, d_out = (
+        query[0], keys[0], values[0], output[0], cum[0], d_out[0]
+    )
+    length, width = query.shape
+    heads = cum.shape[0]
+    head_width = width // heads
+    per_group = LANES // head_width
+    tokens, model = d_out.shape
+    block_rows = w_out.shape[0]
+    attn = output.shape[1]
+    piece_rows = block_rows // split
+
+    def device(shard, group):
+        return shard * groups + group
+
+    def sp_swap(array, step):
+        return lax.ppermute(array, "sp", [(i, i ^ step) for i in range(split)])
+
+    def inner_swap(array):
+        return lax.ppermute(array, "dp", [(i, i ^ 1) for i in range(groups)])
+
+    def outer_shift(array, step):
+        pairs = []
+        for outer in range(split):
+            for at in range(inner):
+                pairs.append((outer * inner + at, (outer + step) % split * inner + at))
+        return lax.ppermute(array, "dp", pairs)
+
+    first_rows = []
+    for step in range(split):
+        pairs = []
+        for shard in range(split):
+            for at in range(inner):
+                for replica in range(split):
+                    source = device(replica, shard * inner + at)
+                    pairs.append((source, device(shard, (replica + step) % split * inner + at)))
+        piece = w_out[step * piece_rows : (step + 1) * piece_rows]
+        first_rows.append(lax.ppermute(piece, ("sp", "dp"), pairs))
+
+    far = sp_swap(d_out, 2)
+    shards = [d_out, sp_swap(d_out, 1), far, sp_swap(far, 1)]
+
+    second_rows = [inner_swap(piece) for piece in first_rows]
+
+    prob, out_t, keys_t = call(
+        functools.partial(prob_kernel, heads),
+        [((heads, length, length), BF16), ((attn, length), BF16), ((width, length), BF16)],
+        (query, keys, output, cum),
+    )
+    share = (split, block_rows, model // split)
+    keep, send = call(
+        functools.partial(weight_kernel, inner),
+        [(share, F32), (share, BF16)],
+        (out_t, *shards),
+        [((length, model // split), BF16)],
+    )
+    got = inner_swap(send)
+    own, *parts = call(
+        merge_kernel, [(share[1:], F32)] + [(share[1:], BF16)] * (split - 1), (keep, got)
+    )
+    parts = [outer_shift(part, step) for step, part in enumerate(parts, 1)]
+    grad_weight, = call(finish_kernel, [(share[1:], F32)], (own, *parts))
+
+    slot = (3, tokens, LANES)
+    arrived, cums = [], []
+    for other, rows in ((False, first_rows), (True, second_rows)):
+        *slots, part_cum = call(
+            functools.partial(grads_kernel, other, heads, split, split),
+            [(slot, BF16)] * split + [((per_group, length), F32)],
+            (prob, query, keys_t, values, out_t, *shards, *rows),
+            [
+                ((LANES, length), BF16),
+                ((length, length), BF16),
+                ((length, LANES), BF16),
+                ((length, LANES), BF16),
+                ((length, LANES), BF16),
+                ((length, LANES), F32),
+            ],
+        )
+        arrived.append([slots[0]] + [sp_swap(slots[i], i) for i in range(1, split)])
+        cums.append(part_cum)
+    query_grad, key_grad, value_grad, cum_grad = call(
+        functools.partial(place_kernel, split),
+        [((tokens, attn), BF16)] * 3 + [((heads, length), F32)],
+        (*arrived[0], *arrived[1], *cums),
+    )
+    return query_grad[None], key_grad[None], value_grad[None], cum_grad[None], grad_weight
 
 
 def head_grads(query, keys, values, output, cotangent, cum):
@@ -107,6 +388,28 @@
     return (query_grad, key_grad, value_grad, grads[3][None], grad_weight)
 
 
+def fits(sizes, args):
+    split, groups = sizes
+    query, output, cum, d_out, w_out = args[0], args[3], args[4], args[5], args[6]
+    length, attn = query.shape[1:]
+    width, heads = attn // split, cum.shape[1] // split
+    head_width = width // max(heads, 1)
+    return (
+        split == 4
+        and groups == 2 * split
+        and width == 2 * LANES
+        and heads * head_width == width
+        and LANES % head_width == 0
+        and 8 % heads == 0
+        and head_width**0.5 % 1 == 0
+        and head_width & (head_width - 1) == 0
+        and w_out.shape[0] // groups == LANES
+        and output.shape[2] == attn
+        and d_out.shape[1] // split == LANES
+        and d_out.shape[2] % (split * LANES) == 0
+    )
+
+
 def solution(mesh):
     placed = (
         P("dp", None, "sp"),
@@ -117,16 +420,22 @@
         P("dp", "sp", None),
         P("dp", None),
     )
-    return jax.shard_map(
-        shards,
-        mesh=mesh,
-        in_specs=placed,
-        out_specs=(
-            P("dp", "sp", None),
-            P("dp", "sp", None),
-            P("dp", "sp", None),
-            P("dp", "sp", None),
-            P("dp", "sp"),
-        ),
-        check_vma=False,
-    )
+    sizes = (mesh.shape["sp"], mesh.shape["dp"])
+
+    def step(*args):
+        body = functools.partial(fused_shards, sizes) if fits(sizes, args) else shards
+        return jax.shard_map(
+            body,
+            mesh=mesh,
+            in_specs=placed,
+            out_specs=(
+                P("dp", "sp", None),
+                P("dp", "sp", None),
+                P("dp", "sp", None),
+                P("dp", "sp", None),
+                P("dp", "sp"),
+            ),
+            check_vma=False,
+        )(*args)
+
+    return step

time: 164 us -> 81.3 us (0.50)
  waiting for transfers between devices: 67.7 us -> 19.3 us
  Pallas kernels: 0 us -> 26.2 us
  other arithmetic: 21.9 us -> 0 us
  matrix products: 17.1 us -> 0 us
  starting transfers between devices: 13.9 us -> 30.3 us
  between operations: 14.5 us -> 0.78 us
  blocking collectives: 12.9 us -> 0 us
  local copies, waits for them, and re-layouts: 15.5 us -> 4.48 us
    all_gather x1 -> x0, waiting for transfers between devices: 45.8 us -> none  [shards(): lax.all_gather(w_out, 'dp', axis=0, tiled=True)]
    ppermute x0 -> x21, starting transfers between devices: none -> 30.3 us  [the longest x9 12.1 us: sp_swap(): return lax.ppermute(array, 'sp', [(i, i ^ step) for i in range(split)])]
    pallas_call x0 -> x7, Pallas kernels: none -> 26.2 us  [call(): pl.pallas_call(kernel, out_shape=[jax.ShapeDtypeStruct(shape, kind) for s...]
    unnamed x5 -> x0, other arithmetic: 21.1 us -> none
    ppermute x0 -> x21, waiting for transfers between devices: none -> 19.3 us  [the longest x9 17.4 us: sp_swap(): return lax.ppermute(array, 'sp', [(i, i ^ step) for i in range(split)])]
    reduce_scatter x1 -> x0, waiting for transfers between devices: 14.2 us -> none  [shards(): lax.psum_scatter(lax.dot_general(whole_output, column_part[0], (((0,), (0...]
    all_to_all x4 -> x0, starting transfers between devices: 13.8 us -> none  [the longest x1 3.6 us: shards(): lax.all_to_all(d_attn[None], 'sp', split_axis=2, concat_axis=1, tiled=True)]
    dot_general x6 -> x0, matrix products: 13.7 us -> none  [the longest x4 7.92 us: product(): return jnp.einsum(form, left, right, preferred_element_type=jnp.float32)]
  transfers between devices with their start and end apart: 6 -> 21, of which waited for: 5 -> 4; matrix products, arithmetic and copies ran while one was open for 33% -> 0% of each run, Pallas kernels for 0% -> 25%
where the time goes in v1:
time: 81.3 us; the launch traced here: 81.1 us
  starting transfers between devices  30.3 us (37%)
  Pallas kernels  26.2 us (32%)
  waiting for transfers between devices  19.3 us (24%)
  local copies, waits for them, and re-layouts  4.48 us (6%)
    pallas_call x7, Pallas kernels, call(): pl.pallas_call(kernel, out_shape=[jax.ShapeDtypeStruct(shape, kind) for s...  26.2 us
    ppermute x9, waiting for transfers between devices, sp_swap(): return lax.ppermute(array, 'sp', [(i, i ^ step) for i in range(split)])  17.4 us
    ppermute x9, starting transfers between devices, sp_swap(): return lax.ppermute(array, 'sp', [(i, i ^ step) for i in range(split)])  12.1 us
    ppermute x4, starting transfers between devices, fused_shards(): first_rows.append(lax.ppermute(piece, ('sp', 'dp'), pairs))  9.57 us
    ppermute x5, starting transfers between devices, inner_swap(): return lax.ppermute(array, 'dp', [(i, i ^ 1) for i in range(groups)])  4.82 us
    unnamed x44, local copies, waits for them, and re-layouts  4.44 us
    ppermute x3, starting transfers between devices, outer_shift(): return lax.ppermute(array, 'dp', pairs)  3.9 us
    ppermute x4, waiting for transfers between devices, fused_shards(): first_rows.append(lax.ppermute(piece, ('sp', 'dp'), pairs))  1.82 us
  transfers between devices with their start and end apart: 21, of which 4 were waited for; matrix products, arithmetic and copies ran while one was open for 0% of the time, Pallas kernels for 25%

profile of v1, /device:TPU:0, one launch (start us, length us, event | category | flops | bytes accessed | tf_op | source)
XLA Modules:
  0.0 81.1 jit_solution(12928510662796425303)
XLA Ops:
  0.6 3.0 %collective-permute-start.1 = (bf16[128,2048]{1,0:T(8,128)(2,1)}, bf16[128,2048]{1,0:T(8,128)(2,1)S(1)}, u32[]{:S(2)}, u32[]{:S(2)}) collective-permute-start(bf16[128,2048]{1,0:T(8,128)(2,1)} %bitcast.10), channel_id=1, source_target_pairs={{0,16},{8,24},{16,0},{24,8},{1,17},{9,25},{17,1},{25,9},{2,18},{10... | collective-permute-start | bytes 1572872 | tf_op jit(solution)/shard_map/ppermute | solution.py:215
  3.7 12.1 %collective-permute-done.1.refs_7_.refs_3_ = bf16[128,2048]{1,0:T(8,128)(2,1)S(1)} collective-permute-done((bf16[128,2048]{1,0:T(8,128)(2,1)}, bf16[128,2048]{1,0:T(8,128)(2,1)S(1)}, u32[]{:S(2)}, u32[]{:S(2)}) %collective-permute-start.1) | collective-permute-done | bytes 524320 | tf_op jit(solution)/shard_map/ppermute | solution.py:215
  15.8 4.8 %shard_map.110 = (bf16[4,512,512]{2,1,0:T(8,128)(2,1)}, bf16[1024,512]{1,0:T(8,128)(2,1)}, bf16[256,512]{1,0:T(8,128)(2,1)}) custom-call(bf16[512,256]{1,0:T(8,128)(2,1)} %bitcast.15, bf16[512,256]{1,0:T(8,128)(2,1)} %bitcast.21, bf16[512,1024]{1,0:T(8,128)(2,1)} %bitcast.20, f32[4,512]{1,0:T(4,128)} %bitcast.22), custom_call_target="tpu_custom_call" | custom-call | tf_op jit(solution)/shard_map/pallas_call | solution.py:187
  20.6 0.8 copy-done.1
  21.6 3.7 %shard_map.114 = (f32[4,128,512]{2,1,0:T(8,128)}, bf16[4,128,512]{2,1,0:T(8,128)(2,1)}) custom-call(bf16[1024,512]{1,0:T(8,128)(2,1)} %get-tuple-element.30.refs_4_.refs_0_, bf16[128,2048]{1,0:T(8,128)(2,1)} %bitcast.12, bf16[128,2048]{1,0:T(8,128)(2,1)} %copy-done.1, bf16[128,2048]{1,0:T(8,128)(2,1)} %copy-done, bf16[128,2048]{1,0:T(8,128)(2,1)} %copy-done.2), custom_call_target="tpu_custom_call" | custom-call | tf_op jit(solution)/shard_map/pallas_call | solution.py:187
  25.3 1.8 %collective-permute-start.17 = (bf16[4,128,512]{2,1,0:T(8,128)(2,1)}, bf16[4,128,512]{2,1,0:T(8,128)(2,1)S(1)}, u32[]{:S(2)}, u32[]{:S(2)}) collective-permute-start(bf16[4,128,512]{2,1,0:T(8,128)(2,1)} %get-tuple-element.46), channel_id=1, source_target_pairs={{0,1},{1,0},{2,3},{3,2},{4,5},{5,4},{6,7},{7,6},{8,9},{9,8},{10,11... | collective-permute-start | bytes 1572872 | tf_op jit(solution)/shard_map/ppermute | solution.py:218
  27.1 0.7 collective-permute-start.3
  27.8 3.0 %collective-permute-start.4 = (bf16[32,2048]{1,0:T(8,128)(2,1)S(1)}, bf16[32,2048]{1,0:T(8,128)(2,1)S(1)}, u32[]{:S(2)}, u32[]{:S(2)}) collective-permute-start(bf16[32,2048]{1,0:T(8,128)(2,1)S(1)} %get-tuple-element.52), channel_id=1, source_target_pairs={{0,2},{8,4},{16,6},{24,0},{1,3},{9,5},{17,7},{25,1},{2,10},{10,12}... | collective-permute-start | bytes 393224 | tf_op jit(solution)/shard_map/ppermute | solution.py:236
  30.8 3.5 %collective-permute-start.5 = (bf16[32,2048]{1,0:T(8,128)(2,1)S(1)}, bf16[32,2048]{1,0:T(8,128)(2,1)S(1)}, u32[]{:S(2)}, u32[]{:S(2)}) collective-permute-start(bf16[32,2048]{1,0:T(8,128)(2,1)S(1)} %get-tuple-element.54), channel_id=1, source_target_pairs={{0,4},{8,6},{16,0},{24,2},{1,5},{9,7},{17,1},{25,3},{2,12},{10,14}... | collective-permute-start | bytes 393224 | tf_op jit(solution)/shard_map/ppermute | solution.py:236
  34.2 2.4 %collective-permute-start.6 = (bf16[32,2048]{1,0:T(8,128)(2,1)S(1)}, bf16[32,2048]{1,0:T(8,128)(2,1)S(1)}, u32[]{:S(2)}, u32[]{:S(2)}) collective-permute-start(bf16[32,2048]{1,0:T(8,128)(2,1)S(1)} %get-tuple-element.51), channel_id=1, source_target_pairs={{0,6},{8,0},{16,2},{24,4},{1,7},{9,1},{17,3},{25,5},{2,14},{10,8},... | collective-permute-start | bytes 393224 | tf_op jit(solution)/shard_map/ppermute | solution.py:236
  37.2 1.8 %collective-permute-done.4.refs_10_ = bf16[32,2048]{1,0:T(8,128)(2,1)S(1)} collective-permute-done((bf16[32,2048]{1,0:T(8,128)(2,1)S(1)}, bf16[32,2048]{1,0:T(8,128)(2,1)S(1)}, u32[]{:S(2)}, u32[]{:S(2)}) %collective-permute-start.4) | collective-permute-done | bytes 131104 | tf_op jit(solution)/shard_map/ppermute | solution.py:236
  39.0 0.5 collective-permute-start.11
  39.5 1.5 %collective-permute-start.12 = (bf16[32,2048]{1,0:T(8,128)(2,1)S(1)}, bf16[32,2048]{1,0:T(8,128)(2,1)S(1)}, u32[]{:S(2)}, u32[]{:S(2)}) collective-permute-start(bf16[32,2048]{1,0:T(8,128)(2,1)S(1)} %collective-permute-done.5.refs_11_), channel_id=1, source_target_pairs={{0,1},{1,0},{2,3},{3,2},{4,5},{5,4},{6,7},{7,6},{8,9},{9,8},{10,11... | collective-permute-start | bytes 393224 | tf_op jit(solution)/shard_map/ppermute | solution.py:218
  41.0 0.5 collective-permute-start.13
  41.7 5.7 %shard_map.111 = (bf16[3,128,128]{2,1,0:T(8,128)(2,1)}, bf16[3,128,128]{2,1,0:T(8,128)(2,1)}, bf16[3,128,128]{2,1,0:T(8,128)(2,1)}, bf16[3,128,128]{2,1,0:T(8,128)(2,1)}, f32[2,512]{1,0:T(2,128)}) custom-call(bf16[4,512,512]{2,1,0:T(8,128)(2,1)} %get-tuple-element.28.refs_0_, bf16[512,256]{1,0:T(8,128)(2,1)} %bitcast.16, ...), custom_call_target="tpu_custom_call" | custom-call | tf_op jit(solution)/shard_map/pallas_call | solution.py:187
  47.4 1.8 %collective-permute-start.7 = (bf16[3,128,128]{2,1,0:T(8,128)(2,1)}, bf16[3,128,128]{2,1,0:T(8,128)(2,1)S(1)}, u32[]{:S(2)}, u32[]{:S(2)}) collective-permute-start(bf16[3,128,128]{2,1,0:T(8,128)(2,1)} %get-tuple-element.32), channel_id=1, source_target_pairs={{0,8},{8,0},{16,24},{24,16},{1,9},{9,1},{17,25},{25,17},{2,10},{10... | collective-permute-start | bytes 294920 | tf_op jit(solution)/shard_map/ppermute | solution.py:215
  49.1 5.6 %collective-permute-start.8 = (bf16[3,128,128]{2,1,0:T(8,128)(2,1)}, bf16[3,128,128]{2,1,0:T(8,128)(2,1)S(1)}, u32[]{:S(2)}, u32[]{:S(2)}) collective-permute-start(bf16[3,128,128]{2,1,0:T(8,128)(2,1)} %get-tuple-element.33), channel_id=1, source_target_pairs={{0,16},{8,24},{16,0},{24,8},{1,17},{9,25},{17,1},{25,9},{2,18},{10... | collective-permute-start | bytes 294920 | tf_op jit(solution)/shard_map/ppermute | solution.py:215
  54.9 0.5 copy-done.12
  55.4 0.6 copy-done.15
  56.1 5.7 %shard_map.112 = (bf16[3,128,128]{2,1,0:T(8,128)(2,1)}, bf16[3,128,128]{2,1,0:T(8,128)(2,1)}, bf16[3,128,128]{2,1,0:T(8,128)(2,1)}, bf16[3,128,128]{2,1,0:T(8,128)(2,1)}, f32[2,512]{1,0:T(2,128)}) custom-call(bf16[4,512,512]{2,1,0:T(8,128)(2,1)} %get-tuple-element.28.refs_0_, bf16[512,256]{1,0:T(8,128)(2,1)} %bitcast.17, ...), custom_call_target="tpu_custom_call" | custom-call | tf_op jit(solution)/shard_map/pallas_call | solution.py:187
  61.9 0.8 copy-done.3
  62.7 2.2 %shard_map.115 = (f32[128,512]{1,0:T(8,128)}, bf16[128,512]{1,0:T(8,128)(2,1)}, bf16[128,512]{1,0:T(8,128)(2,1)}, bf16[128,512]{1,0:T(8,128)(2,1)}) custom-call(f32[4,128,512]{2,1,0:T(8,128)} %get-tuple-element.45.keep_ref, bf16[4,128,512]{2,1,0:T(8,128)(2,1)} %copy-done.3), custom_call_target="tpu_custom_call" | custom-call | tf_op jit(solution)/shard_map/pallas_call | solution.py:187
  64.9 1.0 %collective-permute-start.18 = (bf16[128,512]{1,0:T(8,128)(2,1)}, bf16[128,512]{1,0:T(8,128)(2,1)S(1)}, u32[]{:S(2)}, u32[]{:S(2)}) collective-permute-start(bf16[128,512]{1,0:T(8,128)(2,1)} %get-tuple-element.48), channel_id=1, source_target_pairs={{0,2},{1,3},{2,4},{3,5},{4,6},{5,7},{6,0},{7,1},{8,10},{9,11},{10,... | collective-permute-start | bytes 393224 | tf_op jit(solution)/shard_map/ppermute | solution.py:225
  65.8 1.4 %collective-permute-start.19 = (bf16[128,512]{1,0:T(8,128)(2,1)}, bf16[128,512]{1,0:T(8,128)(2,1)S(1)}, u32[]{:S(2)}, u32[]{:S(2)}) collective-permute-start(bf16[128,512]{1,0:T(8,128)(2,1)} %get-tuple-element.49), channel_id=1, source_target_pairs={{0,4},{1,5},{2,6},{3,7},{4,0},{5,1},{6,2},{7,3},{8,12},{9,13},{10,... | collective-permute-start | bytes 393224 | tf_op jit(solution)/shard_map/ppermute | solution.py:225
  67.2 1.6 %collective-permute-start.20 = (bf16[128,512]{1,0:T(8,128)(2,1)}, bf16[128,512]{1,0:T(8,128)(2,1)S(1)}, u32[]{:S(2)}, u32[]{:S(2)}) collective-permute-start(bf16[128,512]{1,0:T(8,128)(2,1)} %get-tuple-element.50), channel_id=1, source_target_pairs={{0,6},{1,7},{2,0},{3,1},{4,2},{5,3},{6,4},{7,5},{8,14},{9,15},{10,... | collective-permute-start | bytes 393224 | tf_op jit(solution)/shard_map/ppermute | solution.py:225
  68.8 1.4 %collective-permute-start.15 = (bf16[3,128,128]{2,1,0:T(8,128)(2,1)}, bf16[3,128,128]{2,1,0:T(8,128)(2,1)S(1)}, u32[]{:S(2)}, u32[]{:S(2)}) collective-permute-start(bf16[3,128,128]{2,1,0:T(8,128)(2,1)} %get-tuple-element.37), channel_id=1, source_target_pairs={{0,16},{8,24},{16,0},{24,8},{1,17},{9,25},{17,1},{25,9},{2,18},{10... | collective-permute-start | bytes 294920 | tf_op jit(solution)/shard_map/ppermute | solution.py:215
  70.2 3.7 %collective-permute-done.15.refs_6_ = bf16[3,128,128]{2,1,0:T(8,128)(2,1)S(1)} collective-permute-done((bf16[3,128,128]{2,1,0:T(8,128)(2,1)}, bf16[3,128,128]{2,1,0:T(8,128)(2,1)S(1)}, u32[]{:S(2)}, u32[]{:S(2)}) %collective-permute-start.15) | collective-permute-done | bytes 98336 | tf_op jit(solution)/shard_map/ppermute | solution.py:215
  73.9 1.6 %collective-permute-done.16.refs_7_ = bf16[3,128,128]{2,1,0:T(8,128)(2,1)S(1)} collective-permute-done((bf16[3,128,128]{2,1,0:T(8,128)(2,1)}, bf16[3,128,128]{2,1,0:T(8,128)(2,1)S(1)}, u32[]{:S(2)}, u32[]{:S(2)}) %collective-permute-start.16) | collective-permute-done | bytes 98336 | tf_op jit(solution)/shard_map/ppermute | solution.py:215
  75.5 0.6 copy-done.21
  76.1 2.3 %shard_map.113 = (bf16[128,1024]{1,0:T(8,128)(2,1)}, bf16[128,1024]{1,0:T(8,128)(2,1)}, bf16[128,1024]{1,0:T(8,128)(2,1)}, f32[4,512]{1,0:T(4,128)}) custom-call(bf16[3,128,128]{2,1,0:T(8,128)(2,1)} %get-tuple-element.31.refs_0_, bf16[3,128,128]{2,1,0:T(8,128)(2,1)} %copy-done.16, bf16[3,128,128]{2,1,0:T(8,128)(2,1)} %copy-done.17, ...), custom_call_target="tpu_custom_call" | custom-call | tf_op jit(solution)/shard_map/pallas_call | solution.py:187
  78.5 0.6 copy-done.5
  79.2 1.9 %shard_map.116 = f32[128,512]{1,0:T(8,128)} custom-call(f32[128,512]{1,0:T(8,128)} %get-tuple-element.47.own_ref, bf16[128,512]{1,0:T(8,128)(2,1)} %copy-done.5, bf16[128,512]{1,0:T(8,128)(2,1)} %copy-done.7, bf16[128,512]{1,0:T(8,128)(2,1)} %copy-done.11), custom_call_target="tpu_custom_call" | custom-call | tf_op jit(solution)/shard_map/pallas_call | solution.py:187
  (62 shorter events, 1.3 us)
Async XLA Ops:
  0.6 15.2 %collective-permute-start.1 = (bf16[128,2048]{1,0:T(8,128)(2,1)}, bf16[128,2048]{1,0:T(8,128)(2,1)S(1)}, u32[]{:S(2)}, u32[]{:S(2)}) collective-permute-start(bf16[128,2048]{1,0:T(8,128)(2,1)} %bitcast.10), channel_id=1, source_target_pairs={{0,16},{8,24},{16,0},{24,8},{1,17},{9,25},{17,1},{25,9},{2,18},{10... | collective-permute-start | bytes 1572872 | tf_op jit(solution)/shard_map/ppermute | solution.py:215
  3.7 16.9 %collective-permute-start = (bf16[128,2048]{1,0:T(8,128)(2,1)}, bf16[128,2048]{1,0:T(8,128)(2,1)S(1)}, u32[]{:S(2)}, u32[]{:S(2)}) collective-permute-start(bf16[128,2048]{1,0:T(8,128)(2,1)} %bitcast.11), channel_id=1, source_target_pairs={{0,8},{8,0},{16,24},{24,16},{1,9},{9,1},{17,25},{25,17},{2,10},{10... | collective-permute-start | bytes 1572872 | tf_op jit(solution)/shard_map/ppermute | solution.py:215
  15.8 4.8 %copy-start = (bf16[128,2048]{1,0:T(8,128)(2,1)}, bf16[128,2048]{1,0:T(8,128)(2,1)S(1)}, u32[]{:S(2)}) copy-start(bf16[128,2048]{1,0:T(8,128)(2,1)S(1)} %collective-permute-done.1.refs_7_.refs_3_) | copy-start | bytes 1572868
  15.8 4.8 %collective-permute-start.2 = (bf16[128,2048]{1,0:T(8,128)(2,1)S(1)}, bf16[128,2048]{1,0:T(8,128)(2,1)S(1)}, u32[]{:S(2)}, u32[]{:S(2)}) collective-permute-start(bf16[128,2048]{1,0:T(8,128)(2,1)S(1)} %collective-permute-done.1.refs_7_.refs_3_), channel_id=1, source_target_pairs={{0,8},{8,0},{16,24},{24,16},{1,9},{9,1},{17,25},{25,17},{2,10},{10... | collective-permute-start | bytes 1572872 | tf_op jit(solution)/shard_map/ppermute | solution.py:215
  15.8 11.2 %copy-start.4 = (bf16[128,2048]{1,0:T(8,128)(2,1)S(1)}, bf16[128,2048]{1,0:T(8,128)(2,1)}, u32[]{:S(2)}) copy-start(bf16[128,2048]{1,0:T(8,128)(2,1)} %param.13) | copy-start | bytes 1572868
  25.3 36.6 %collective-permute-start.17 = (bf16[4,128,512]{2,1,0:T(8,128)(2,1)}, bf16[4,128,512]{2,1,0:T(8,128)(2,1)S(1)}, u32[]{:S(2)}, u32[]{:S(2)}) collective-permute-start(bf16[4,128,512]{2,1,0:T(8,128)(2,1)} %get-tuple-element.46), channel_id=1, source_target_pairs={{0,1},{1,0},{2,3},{3,2},{4,5},{5,4},{6,7},{7,6},{8,9},{9,8},{10,11... | collective-permute-start | bytes 1572872 | tf_op jit(solution)/shard_map/ppermute | solution.py:218
  27.1 9.6 %collective-permute-start.3 = (bf16[32,2048]{1,0:T(8,128)(2,1)S(1)}, bf16[32,2048]{1,0:T(8,128)(2,1)S(1)}, u32[]{:S(2)}, u32[]{:S(2)}) collective-permute-start(bf16[32,2048]{1,0:T(8,128)(2,1)S(1)} %get-tuple-element.53), channel_id=1, source_target_pairs={{0,0},{8,2},{16,4},{24,6},{1,1},{9,3},{17,5},{25,7},{2,8},{10,10},... | collective-permute-start | bytes 393224 | tf_op jit(solution)/shard_map/ppermute | solution.py:236
  27.8 11.2 %collective-permute-start.4 = (bf16[32,2048]{1,0:T(8,128)(2,1)S(1)}, bf16[32,2048]{1,0:T(8,128)(2,1)S(1)}, u32[]{:S(2)}, u32[]{:S(2)}) collective-permute-start(bf16[32,2048]{1,0:T(8,128)(2,1)S(1)} %get-tuple-element.52), channel_id=1, source_target_pairs={{0,2},{8,4},{16,6},{24,0},{1,3},{9,5},{17,7},{25,1},{2,10},{10,12}... | collective-permute-start | bytes 393224 | tf_op jit(solution)/shard_map/ppermute | solution.py:236
  30.8 8.7 %collective-permute-start.5 = (bf16[32,2048]{1,0:T(8,128)(2,1)S(1)}, bf16[32,2048]{1,0:T(8,128)(2,1)S(1)}, u32[]{:S(2)}, u32[]{:S(2)}) collective-permute-start(bf16[32,2048]{1,0:T(8,128)(2,1)S(1)} %get-tuple-element.54), channel_id=1, source_target_pairs={{0,4},{8,6},{16,0},{24,2},{1,5},{9,7},{17,1},{25,3},{2,12},{10,14}... | collective-permute-start | bytes 393224 | tf_op jit(solution)/shard_map/ppermute | solution.py:236
  34.2 6.8 %collective-permute-start.6 = (bf16[32,2048]{1,0:T(8,128)(2,1)S(1)}, bf16[32,2048]{1,0:T(8,128)(2,1)S(1)}, u32[]{:S(2)}, u32[]{:S(2)}) collective-permute-start(bf16[32,2048]{1,0:T(8,128)(2,1)S(1)} %get-tuple-element.51), channel_id=1, source_target_pairs={{0,6},{8,0},{16,2},{24,4},{1,7},{9,1},{17,3},{25,5},{2,14},{10,8},... | collective-permute-start | bytes 393224 | tf_op jit(solution)/shard_map/ppermute | solution.py:236
  36.7 4.9 %copy-start.14 = (bf16[32,2048]{1,0:T(8,128)(2,1)}, bf16[32,2048]{1,0:T(8,128)(2,1)S(1)}, u32[]{:S(2)}) copy-start(bf16[32,2048]{1,0:T(8,128)(2,1)S(1)} %collective-permute-done.3.refs_9_) | copy-start | bytes 393220
  36.7 10.7 %collective-permute-start.10 = (bf16[32,2048]{1,0:T(8,128)(2,1)S(1)}, bf16[32,2048]{1,0:T(8,128)(2,1)S(1)}, u32[]{:S(2)}, u32[]{:S(2)}) collective-permute-start(bf16[32,2048]{1,0:T(8,128)(2,1)S(1)} %collective-permute-done.3.refs_9_), channel_id=1, source_target_pairs={{0,1},{1,0},{2,3},{3,2},{4,5},{5,4},{6,7},{7,6},{8,9},{9,8},{10,11... | collective-permute-start | bytes 393224 | tf_op jit(solution)/shard_map/ppermute | solution.py:218
  39.0 2.6 %copy-start.13 = (bf16[32,2048]{1,0:T(8,128)(2,1)}, bf16[32,2048]{1,0:T(8,128)(2,1)S(1)}, u32[]{:S(2)}) copy-start(bf16[32,2048]{1,0:T(8,128)(2,1)S(1)} %collective-permute-done.4.refs_10_) | copy-start | bytes 393220
  39.0 10.1 %collective-permute-start.11 = (bf16[32,2048]{1,0:T(8,128)(2,1)S(1)}, bf16[32,2048]{1,0:T(8,128)(2,1)S(1)}, u32[]{:S(2)}, u32[]{:S(2)}) collective-permute-start(bf16[32,2048]{1,0:T(8,128)(2,1)S(1)} %collective-permute-done.4.refs_10_), channel_id=1, source_target_pairs={{0,1},{1,0},{2,3},{3,2},{4,5},{5,4},{6,7},{7,6},{8,9},{9,8},{10,11... | collective-permute-start | bytes 393224 | tf_op jit(solution)/shard_map/ppermute | solution.py:218
  39.5 2.0 %copy-start.10 = (bf16[32,2048]{1,0:T(8,128)(2,1)}, bf16[32,2048]{1,0:T(8,128)(2,1)S(1)}, u32[]{:S(2)}) copy-start(bf16[32,2048]{1,0:T(8,128)(2,1)S(1)} %collective-permute-done.5.refs_11_) | copy-start | bytes 393220
  39.5 15.2 %collective-permute-start.12 = (bf16[32,2048]{1,0:T(8,128)(2,1)S(1)}, bf16[32,2048]{1,0:T(8,128)(2,1)S(1)}, u32[]{:S(2)}, u32[]{:S(2)}) collective-permute-start(bf16[32,2048]{1,0:T(8,128)(2,1)S(1)} %collective-permute-done.5.refs_11_), channel_id=1, source_target_pairs={{0,1},{1,0},{2,3},{3,2},{4,5},{5,4},{6,7},{7,6},{8,9},{9,8},{10,11... | collective-permute-start | bytes 393224 | tf_op jit(solution)/shard_map/ppermute | solution.py:218
  41.0 13.8 %collective-permute-start.13 = (bf16[32,2048]{1,0:T(8,128)(2,1)S(1)}, bf16[32,2048]{1,0:T(8,128)(2,1)S(1)}, u32[]{:S(2)}, u32[]{:S(2)}) collective-permute-start(bf16[32,2048]{1,0:T(8,128)(2,1)S(1)} %collective-permute-done.6.refs_12_), channel_id=1, source_target_pairs={{0,1},{1,0},{2,3},{3,2},{4,5},{5,4},{6,7},{7,6},{8,9},{9,8},{10,11... | collective-permute-start | bytes 393224 | tf_op jit(solution)/shard_map/ppermute | solution.py:218
  47.3 7.5 %copy-start.6 = (bf16[32,2048]{1,0:T(8,128)(2,1)}, bf16[32,2048]{1,0:T(8,128)(2,1)S(1)}, u32[]{:S(2)}) copy-start(bf16[32,2048]{1,0:T(8,128)(2,1)S(1)} %collective-permute-done.10.refs_9_) | copy-start | bytes 393220
  47.4 18.5 %collective-permute-start.7 = (bf16[3,128,128]{2,1,0:T(8,128)(2,1)}, bf16[3,128,128]{2,1,0:T(8,128)(2,1)S(1)}, u32[]{:S(2)}, u32[]{:S(2)}) collective-permute-start(bf16[3,128,128]{2,1,0:T(8,128)(2,1)} %get-tuple-element.32), channel_id=1, source_target_pairs={{0,8},{8,0},{16,24},{24,16},{1,9},{9,1},{17,25},{25,17},{2,10},{10... | collective-permute-start | bytes 294920 | tf_op jit(solution)/shard_map/ppermute | solution.py:215
  49.1 5.7 %copy-start.8 = (bf16[32,2048]{1,0:T(8,128)(2,1)}, bf16[32,2048]{1,0:T(8,128)(2,1)S(1)}, u32[]{:S(2)}) copy-start(bf16[32,2048]{1,0:T(8,128)(2,1)S(1)} %collective-permute-done.11.refs_10_) | copy-start | bytes 393220
  49.1 18.1 %collective-permute-start.8 = (bf16[3,128,128]{2,1,0:T(8,128)(2,1)}, bf16[3,128,128]{2,1,0:T(8,128)(2,1)S(1)}, u32[]{:S(2)}, u32[]{:S(2)}) collective-permute-start(bf16[3,128,128]{2,1,0:T(8,128)(2,1)} %get-tuple-element.33), channel_id=1, source_target_pairs={{0,16},{8,24},{16,0},{24,8},{1,17},{9,25},{17,1},{25,9},{2,18},{10... | collective-permute-start | bytes 294920 | tf_op jit(solution)/shard_map/ppermute | solution.py:215
  54.7 14.0 %collective-permute-start.9 = (bf16[3,128,128]{2,1,0:T(8,128)(2,1)}, bf16[3,128,128]{2,1,0:T(8,128)(2,1)S(1)}, u32[]{:S(2)}, u32[]{:S(2)}) collective-permute-start(bf16[3,128,128]{2,1,0:T(8,128)(2,1)} %get-tuple-element.34), channel_id=1, source_target_pairs={{0,24},{8,16},{16,8},{24,0},{1,25},{9,17},{17,9},{25,1},{2,26},{10... | collective-permute-start | bytes 294920 | tf_op jit(solution)/shard_map/ppermute | solution.py:215
  61.7 8.5 %collective-permute-start.14 = (bf16[3,128,128]{2,1,0:T(8,128)(2,1)}, bf16[3,128,128]{2,1,0:T(8,128)(2,1)S(1)}, u32[]{:S(2)}, u32[]{:S(2)}) collective-permute-start(bf16[3,128,128]{2,1,0:T(8,128)(2,1)} %get-tuple-element.36), channel_id=1, source_target_pairs={{0,8},{8,0},{16,24},{24,16},{1,9},{9,1},{17,25},{25,17},{2,10},{10... | collective-permute-start | bytes 294920 | tf_op jit(solution)/shard_map/ppermute | solution.py:215
  64.9 13.6 %collective-permute-start.18 = (bf16[128,512]{1,0:T(8,128)(2,1)}, bf16[128,512]{1,0:T(8,128)(2,1)S(1)}, u32[]{:S(2)}, u32[]{:S(2)}) collective-permute-start(bf16[128,512]{1,0:T(8,128)(2,1)} %get-tuple-element.48), channel_id=1, source_target_pairs={{0,2},{1,3},{2,4},{3,5},{4,6},{5,7},{6,0},{7,1},{8,10},{9,11},{10,... | collective-permute-start | bytes 393224 | tf_op jit(solution)/shard_map/ppermute | solution.py:225
  65.8 9.6 %copy-start.16 = (bf16[3,128,128]{2,1,0:T(8,128)(2,1)}, bf16[3,128,128]{2,1,0:T(8,128)(2,1)S(1)}, u32[]{:S(2)}) copy-start(bf16[3,128,128]{2,1,0:T(8,128)(2,1)S(1)} %collective-permute-done.7.refs_1_) | copy-start | bytes 294916
  65.8 12.6 %collective-permute-start.19 = (bf16[128,512]{1,0:T(8,128)(2,1)}, bf16[128,512]{1,0:T(8,128)(2,1)S(1)}, u32[]{:S(2)}, u32[]{:S(2)}) collective-permute-start(bf16[128,512]{1,0:T(8,128)(2,1)} %get-tuple-element.49), channel_id=1, source_target_pairs={{0,4},{1,5},{2,6},{3,7},{4,0},{5,1},{6,2},{7,3},{8,12},{9,13},{10,... | collective-permute-start | bytes 393224 | tf_op jit(solution)/shard_map/ppermute | solution.py:225
  67.2 8.3 %copy-start.17 = (bf16[3,128,128]{2,1,0:T(8,128)(2,1)}, bf16[3,128,128]{2,1,0:T(8,128)(2,1)S(1)}, u32[]{:S(2)}) copy-start(bf16[3,128,128]{2,1,0:T(8,128)(2,1)S(1)} %collective-permute-done.8.refs_2_) | copy-start | bytes 294916
  67.2 11.3 %collective-permute-start.20 = (bf16[128,512]{1,0:T(8,128)(2,1)}, bf16[128,512]{1,0:T(8,128)(2,1)S(1)}, u32[]{:S(2)}, u32[]{:S(2)}) collective-permute-start(bf16[128,512]{1,0:T(8,128)(2,1)} %get-tuple-element.50), channel_id=1, source_target_pairs={{0,6},{1,7},{2,0},{3,1},{4,2},{5,3},{6,4},{7,5},{8,14},{9,15},{10,... | collective-permute-start | bytes 393224 | tf_op jit(solution)/shard_map/ppermute | solution.py:225
  68.8 6.7 %copy-start.18 = (bf16[3,128,128]{2,1,0:T(8,128)(2,1)}, bf16[3,128,128]{2,1,0:T(8,128)(2,1)S(1)}, u32[]{:S(2)}) copy-start(bf16[3,128,128]{2,1,0:T(8,128)(2,1)S(1)} %collective-permute-done.9.refs_3_) | copy-start | bytes 294916
  68.8 5.1 %collective-permute-start.15 = (bf16[3,128,128]{2,1,0:T(8,128)(2,1)}, bf16[3,128,128]{2,1,0:T(8,128)(2,1)S(1)}, u32[]{:S(2)}, u32[]{:S(2)}) collective-permute-start(bf16[3,128,128]{2,1,0:T(8,128)(2,1)} %get-tuple-element.37), channel_id=1, source_target_pairs={{0,16},{8,24},{16,0},{24,8},{1,17},{9,25},{17,1},{25,9},{2,18},{10... | collective-permute-start | bytes 294920 | tf_op jit(solution)/shard_map/ppermute | solution.py:215
  70.2 5.3 %copy-start.19 = (bf16[3,128,128]{2,1,0:T(8,128)(2,1)}, bf16[3,128,128]{2,1,0:T(8,128)(2,1)S(1)}, u32[]{:S(2)}) copy-start(bf16[3,128,128]{2,1,0:T(8,128)(2,1)S(1)} %collective-permute-done.14.refs_5_) | copy-start | bytes 294916
  70.2 5.3 %collective-permute-start.16 = (bf16[3,128,128]{2,1,0:T(8,128)(2,1)}, bf16[3,128,128]{2,1,0:T(8,128)(2,1)S(1)}, u32[]{:S(2)}, u32[]{:S(2)}) collective-permute-start(bf16[3,128,128]{2,1,0:T(8,128)(2,1)} %get-tuple-element.38), channel_id=1, source_target_pairs={{0,24},{8,16},{16,8},{24,0},{1,25},{9,17},{17,9},{25,1},{2,26},{10... | collective-permute-start | bytes 294920 | tf_op jit(solution)/shard_map/ppermute | solution.py:215
  (11 other events, 8.9 us)
